TPU v7x, 256 devices: a whole 4x4x8 slice. The times are simulated.
256 devices in a mesh: sp: 64 (over z, x, core), tp: 4 (over y).
Axes of the slice: x: 4, y: 4, z: 8, core: 2. Of those that a mesh axis runs over, the one named last changes fastest.
Arguments:
- residual_in: bfloat16 [65536, 2048], P(('sp', 'tp')), may hold values from -6 to 6
- gate_outer: bfloat16 [65536, 1024], P('sp', 'tp'), may hold values from -6 to 6
- gate_inner: bfloat16 [65536, 1024], P('sp', 'tp'), may hold values from -6 to 6
- conv_input: bfloat16 [65536, 1024], P('sp', 'tp'), may hold values from -6 to 6
- conv_taps: bfloat16 [3, 1024], P(None, 'tp'), may hold values from -5 to 5
- norm_gain: bfloat16 [1024], P('tp'), may hold values from 0.099609375 to 1.8984375
- out_weight: bfloat16 [1024, 2048], P('tp'), may hold values from -0.1875 to 0.1875
- moe_gain: bfloat16 [2048], replicated, may hold values from 0.099609375 to 1.8984375
- expert_ids: int32 [65536, 2], P(('sp', 'tp')), may hold values from 0 to 63, all different within a row; in each aligned block of 256 rows (0 to 255, 256 to 511, ...) at most 16 rows name the same one
- group_prob: float32 [65536], P(('sp', 'tp')), may hold values from 0.3 to 1
- route_prob: float32 [65536, 2], P(('sp', 'tp')), may hold values from 0.1 to 1
- expert_gate: bfloat16 [64, 2048, 512], P('sp'), may hold values from -0.125 to 0.125
- expert_up: bfloat16 [64, 2048, 512], P('sp'), may hold values from -0.125 to 0.125
- expert_down: bfloat16 [64, 512, 2048], P('sp'), may hold values from -0.25 to 0.25
Outputs:
- layer_out: bfloat16 [65536, 2048], P(('sp', 'tp'))
Inputs may be any that keep to these rules, and one draw needn't show every extreme that they name: `expert_ids`: each row names 2 different experts. Within the rows of one device (aligned blocks of 256 rows) no expert is named more than 16 times.
All inputs are finite; a program needn't handle non-finite values.
Results may differ from a plain program's by a relative error of at most 0.0075.
Values may be sent and summed in bfloat16 or wider, within the bound.
A program may use at most 64 MiB of HBM per device.

v0:
```python
import jax
import jax.numpy as jnp
from jax import lax
from jax.sharding import PartitionSpec as P

EPSILON = 1e-06


def from_behind(shard, axis, by):
    devices = lax.axis_size(axis)
    pairs = [(i, i + by) for i in range(devices) if 0 <= i + by < devices]
    return lax.ppermute(shard, axis, pairs)


def rms_norm(values, gain):
    floats = values.astype(jnp.float32)
    factor = lax.rsqrt(jnp.mean(floats * floats, axis=-1, keepdims=True) + EPSILON)
    return floats * factor * gain.astype(jnp.float32)


def body(
    residual_in,
    gate_outer,
    gate_inner,
    conv_input,
    conv_taps,
    norm_gain,
    out_weight,
    moe_gain,
    expert_ids,
    group_prob,
    route_prob,
    expert_gate,
    expert_up,
    expert_down,
):
    seq_rows, channels = conv_input.shape
    taps_count = conv_taps.shape[0]
    inner = gate_inner.astype(jnp.float32) * conv_input.astype(jnp.float32)
    earlier = from_behind(inner[seq_rows - (taps_count - 1) :], "sp", 1)
    padded = jnp.concatenate([earlier, inner], axis=0)
    tap_f = conv_taps.astype(jnp.float32)
    filtered = jnp.zeros((seq_rows, channels), jnp.float32)
    for offset in range(taps_count):
        filtered = filtered + tap_f[offset][None, :] * padded[offset : offset + seq_rows]
    mixed_out = (gate_outer.astype(jnp.float32) * filtered).astype(jnp.bfloat16)
    gathered = lax.all_to_all(mixed_out, "tp", split_axis=0, concat_axis=1, tiled=True)
    full_weight, full_gain = (
        lax.all_gather(out_weight, "tp", axis=0, tiled=True),
        lax.all_gather(norm_gain, "tp", axis=0, tiled=True),
    )
    normed = rms_norm(gathered, full_gain).astype(jnp.bfloat16)
    projected = jnp.dot(normed, full_weight, preferred_element_type=jnp.float32)
    residual = (residual_in.astype(jnp.float32) + projected).astype(jnp.bfloat16)
    routed_in = rms_norm(residual, moe_gain).astype(jnp.bfloat16)
    tok_rows, width = routed_in.shape
    top_count = expert_ids.shape[1]
    local_count = expert_gate.shape[0]
    group_count = lax.axis_size("sp")
    experts_all = local_count * group_count
    capacity = 2 * tok_rows * top_count // experts_all
    slots = tok_rows * top_count
    flat_e = expert_ids.reshape(-1)
    one_hot = (flat_e[:, None] == jnp.arange(experts_all, dtype=jnp.int32)[None, :]).astype(
        jnp.int32
    )
    slot_rank = jnp.sum((jnp.cumsum(one_hot, axis=0) - 1) * one_hot, axis=1)
    owner_dev = flat_e // local_count
    local_slot = flat_e % local_count
    position = (local_slot * group_count + owner_dev) * capacity + slot_rank
    source_slot = (
        jnp.full((experts_all * capacity,), slots, jnp.int32)
        .at[position]
        .set(jnp.arange(slots, dtype=jnp.int32))
    )
    rows_pad = jnp.concatenate([routed_in, jnp.zeros((1, width), jnp.bfloat16)], axis=0)
    outgoing = rows_pad[source_slot // top_count].reshape(local_count, group_count, capacity, width)
    arrived = lax.all_to_all(outgoing, "sp", split_axis=1, concat_axis=1, tiled=True)
    gate_act = jnp.einsum(
        "esrd,edf->esrf", arrived, expert_gate, preferred_element_type=jnp.float32
    )
    up_act = jnp.einsum("esrd,edf->esrf", arrived, expert_up, preferred_element_type=jnp.float32)
    hidden = (jax.nn.silu(gate_act) * up_act).astype(jnp.bfloat16)
    result = jnp.einsum(
        "esrf,efd->esrd", hidden, expert_down, preferred_element_type=jnp.float32
    ).astype(jnp.bfloat16)
    returned = lax.all_to_all(result, "sp", split_axis=1, concat_axis=1, tiled=True)
    slot_out = returned.reshape(-1, width)[position].reshape(tok_rows, top_count, width)
    weights = group_prob[:, None] * route_prob / jnp.sum(route_prob, axis=1, keepdims=True)
    expert_sum = jnp.sum(slot_out.astype(jnp.float32) * weights[:, :, None], axis=1)
    return (residual.astype(jnp.float32) + expert_sum).astype(jnp.bfloat16)


def solution(mesh):
    in_specs = (
        P(("sp", "tp"), None),
        P("sp", "tp"),
        P("sp", "tp"),
        P("sp", "tp"),
        P(None, "tp"),
        P("tp"),
        P("tp", None),
        P(),
        P(("sp", "tp"), None),
        P(("sp", "tp")),
        P(("sp", "tp"), None),
        P("sp", None, None),
        P("sp", None, None),
        P("sp", None, None),
    )
    out_specs = P(("sp", "tp"), None)
    return jax.shard_map(body, mesh=mesh, in_specs=in_specs, out_specs=out_specs, check_vma=False)
```

profile of v0, /device:TPU:2, one launch (start us, length us, event | category | flops | bytes accessed | tf_op | source)
XLA Modules:
  0.0 335.0 jit_solution(17748182596416122300)
XLA Ops:
  7.3 1.3 convert_multiply_fusion.3
  8.6 1.9 collective-permute-start
  11.0 1.2 reduce-window.6
  12.6 10.0 %all-gather = bf16[4,1,256]{2,1,0:T(2,128)(2,1)S(1)} all-gather(bf16[1,1,256]{2,1,0:T(2,128)(2,1)S(1)} %reshape.144), channel_id=1, replica_groups=mesh['sp'=64,'tp'=4] {'tp'}, dimensions={0}, use_global_device_ids=true | all-gather | bytes 2560 | tf_op jit(solution)/shard_map/all_gather | solution.py:50
  23.0 2.3 fusion.25
  25.2 3.5 %all-to-all-start = ((bf16[4,256,256]{2,1,0:T(8,128)(2,1)}), bf16[4,256,256]{2,1,0:T(8,128)(2,1)S(1)}, u32[]{:S(2)}, u32[]{:S(2)}) async-start(bf16[4,256,256]{2,1,0:T(8,128)(2,1)} %bitcast.66), calls=%async_computation | async-start | bytes 1048576 | tf_op jit(solution)/shard_map/all_to_all | solution.py:47
  28.8 2.4 scatter_custom_fusion
  31.2 13.6 %all-to-all-done = bf16[4,256,256]{2,1,0:T(8,128)(2,1)S(1)} async-done(((bf16[4,256,256]{2,1,0:T(8,128)(2,1)}), bf16[4,256,256]{2,1,0:T(8,128)(2,1)S(1)}, u32[]{:S(2)}, u32[]{:S(2)}) %all-to-all-start) | async-done | bytes 524320 | tf_op jit(solution)/shard_map/all_to_all | solution.py:47
  44.8 1.1 convert_bitcast_fusion.1
  45.8 2.5 copy.27
  48.6 1.4 fusion.29
  50.0 18.5 %all-gather.3.cloned.1.call-done = bf16[1024,2048]{1,0:T(8,128)(2,1)} async-done(((bf16[256,2048]{1,0:T(8,128)(2,1)}), bf16[1024,2048]{1,0:T(8,128)(2,1)}) %all-gather.3.cloned.1.call-update) | async-done | bytes 4194320 | tf_op jit(solution)/shard_map/all_gather | solution.py:49
  68.5 3.9 %fusion.5 = (f32[256]{0:T(256)S(1)}, bf16[256,2048]{1,0:T(8,128)(2,1)S(1)}) fusion(bf16[256,1024]{0,1:T(8,128)(2,1)S(1)} %fusion.29, bf16[1024,2048]{1,0:T(8,128)(2,1)} %all-gather.3.cloned.1.call-done, bf16[256,2048]{1,0:T(8,128)(2,1)} %param.14), kind=kOutput, calls=%fused_computation.14 | convolution fusion | flops 1076887296 | bytes 6816768 | tf_op jit(solution)/shard_map/dot_general | solution.py:53
  73.8 6.0 %gather_fusion = bf16[1024,2048]{1,0:T(8,128)(2,1)} fusion(bf16[257,2048]{1,0:T(8,128)(2,1)S(1)} %concatenate.7, s32[1024]{0:T(1024)S(1)} %fusion.35), kind=kCustom, calls=%fused_computation | custom fusion | bytes 8392704 | tf_op jit(solution)/shard_map/gather | solution.py:77
  79.8 106.9 %all_to_all.23 = bf16[1,64,16,2048]{3,2,0,1:T(8,128)(2,1)S(1)} all-to-all(bf16[1,64,16,2048]{3,2,0,1:T(8,128)(2,1)} %bitcast.65), channel_id=1, replica_groups=mesh['sp'=64,'tp'=4] {'sp'}, dimensions={1} | all-to-all | bytes 8388608 | tf_op jit(solution)/shard_map/all_to_all | solution.py:78
  186.7 2.0 copy-done.1
  188.7 3.7 %fusion.2 = f32[64,16,512]{2,1,0:T(8,128)} fusion(bf16[1,64,16,2048]{3,2,0,1:T(8,128)(2,1)S(1)} %all_to_all.23, bf16[1,2048,512]{2,1,0:T(8,128)(2,1)S(1)} %copy-done.9), kind=kOutput, calls=%fused_computation.5 | convolution fusion | flops 2147483648 | bytes 8388608 | tf_op jit(solution)/shard_map/esrd,edf->esrf/dot_general | solution.py:79
  192.4 10.0 %convert_bitcast_fusion = bf16[1,64,16,2048]{3,2,0,1:T(8,128)(2,1)} fusion(bf16[1,512,2048]{2,1,0:T(8,128)(2,1)S(1)} %copy-done, f32[64,16,512]{2,1,0:T(8,128)} %fusion.2, bf16[1,2048,512]{2,1,0:T(8,128)(2,1)} %param.26, bf16[1,64,16,2048]{3,2,0,1:T(8,128)(2,1)} %copy-done.1), kind=kOutput, calls=%fused_computation.8 | convolution fusion | flops 4300210176 | bytes 14680064 | tf_op jit(solution)/shard_map/esrf,efd->esrd/dot_general | solution.py:84
  202.4 5.9 %all-to-all-start.2 = ((bf16[1,64,16,2048]{3,2,0,1:T(8,128)(2,1)}), bf16[1,64,16,2048]{3,2,0,1:T(8,128)(2,1)}, u32[]{:S(2)}, u32[]{:S(2)}) async-start(bf16[1,64,16,2048]{3,2,0,1:T(8,128)(2,1)} %convert_bitcast_fusion), calls=%async_computation.2 | async-start | bytes 8388608 | tf_op jit(solution)/shard_map/all_to_all | solution.py:87
  208.5 96.0 %all-to-all-done.2 = bf16[1,64,16,2048]{3,2,0,1:T(8,128)(2,1)} async-done(((bf16[1,64,16,2048]{3,2,0,1:T(8,128)(2,1)}), bf16[1,64,16,2048]{3,2,0,1:T(8,128)(2,1)}, u32[]{:S(2)}, u32[]{:S(2)}) %all-to-all-start.2) | async-done | bytes 4194336 | tf_op jit(solution)/shard_map/all_to_all | solution.py:87
  304.5 8.0 %gather_fusion.1 = bf16[512,2048]{1,0:T(8,128)(2,1)} fusion(bf16[1024,2048]{1,0:T(8,128)(2,1)} %bitcast.21, s32[1024]{0:T(1024)S(1)} %pad_clamp_fusion), kind=kCustom, calls=%fused_computation.1 | custom fusion | bytes 4196352 | tf_op jit(solution)/shard_map/gather | solution.py:88
  312.5 5.4 %reshape.118 = f32[256,2,2048]{2,1,0:T(2,128)} reshape(bf16[512,2048]{1,0:T(8,128)(2,1)} %gather_fusion.1) | data formatting | bytes 6291456 | tf_op jit(solution)/shard_map/convert_element_type | solution.py:90
  317.9 9.0 %multiply_reduce_fusion = f32[256,2048]{1,0:T(8,128)S(1)} fusion(f32[256,2,2048]{2,1,0:T(2,128)} %reshape.118, f32[256,2]{1,0:T(8,128)S(1)} %copy.34), kind=kLoop, calls=%fused_computation.7 | loop fusion | flops 1572864 | bytes 6293504 | tf_op jit(solution)/shard_map/reduce_sum | solution.py:90
  326.9 1.3 fusion.8
  (52 shorter events, 3.6 us)
Async XLA Ops:
  6.5 185.9 %copy-start = (bf16[1,512,2048]{2,1,0:T(8,128)(2,1)S(1)}, bf16[1,512,2048]{2,1,0:T(8,128)(2,1)}, u32[]{:S(2)}) copy-start(bf16[1,512,2048]{2,1,0:T(8,128)(2,1)} %param.27) | copy-start | bytes 6291460
  6.5 4.0 %copy-start.4 = (s32[256,2]{0,1:T(2,128)S(1)}, s32[256,2]{0,1:T(2,128)}, u32[]{:S(2)}) copy-start(s32[256,2]{0,1:T(2,128)} %param.22) | copy-start | bytes 6148
  6.5 5.9 %copy-start.6 = (bf16[3,256]{1,0:T(4,128)(2,1)S(1)}, bf16[3,256]{1,0:T(4,128)(2,1)}, u32[]{:S(2)}) copy-start(bf16[3,256]{1,0:T(4,128)(2,1)} %param.18) | copy-start | bytes 4612
  6.5 6.1 %copy-start.10 = (bf16[256]{0:T(256)(128)(2,1)S(1)}, bf16[256]{0:T(256)(128)(2,1)}, u32[]{:S(2)}) copy-start(bf16[256]{0:T(256)(128)(2,1)} %param.19) | copy-start | bytes 1540
  6.5 16.1 %copy-start.7 = (bf16[2048]{0:T(1024)(128)(2,1)S(1)}, bf16[2048]{0:T(1024)(128)(2,1)}, u32[]{:S(2)}) copy-start(bf16[2048]{0:T(1024)(128)(2,1)} %param.21) | copy-start | bytes 12292
  6.5 62.0 %all-gather.3.cloned.1.call-start = ((), (), s32[]{:S(2)}) async-start(), calls=%async_computation.3 | async-start | bytes 5242880 | tf_op jit(solution)/shard_map/all_gather | solution.py:49
  8.6 14.3 %collective-permute-start = (f32[2,256]{1,0:T(2,128)S(1)}, f32[2,256]{1,0:T(2,128)S(1)}, u32[]{:S(2)}, u32[]{:S(2)}) collective-permute-start(f32[2,256]{1,0:T(2,128)S(1)} %slice.37), channel_id=1, source_target_pairs={{0,4},{4,8},{8,12},{12,16},{16,20},{20,24},{24,28},{28,32},{32,36}... | collective-permute-start | bytes 6152 | tf_op jit(solution)/shard_map/ppermute | solution.py:12
  25.2 19.5 %all-to-all-start = ((bf16[4,256,256]{2,1,0:T(8,128)(2,1)}), bf16[4,256,256]{2,1,0:T(8,128)(2,1)S(1)}, u32[]{:S(2)}, u32[]{:S(2)}) async-start(bf16[4,256,256]{2,1,0:T(8,128)(2,1)} %bitcast.66), calls=%async_computation | async-start | bytes 1048576 | tf_op jit(solution)/shard_map/all_to_all | solution.py:47
  72.4 1.0 copy-start.2
  79.8 108.8 %copy-start.9 = (bf16[1,2048,512]{2,1,0:T(8,128)(2,1)S(1)}, bf16[1,2048,512]{2,1,0:T(8,128)(2,1)}, u32[]{:S(2)}) copy-start(bf16[1,2048,512]{2,1,0:T(8,128)(2,1)} %param.25) | copy-start | bytes 6291460
  186.7 2.0 copy-start.1
  202.4 5.9 %copy-start.5 = (f32[256,2]{0,1:T(2,128)S(1)}, f32[256,2]{0,1:T(2,128)}, u32[]{:S(2)}) copy-start(f32[256,2]{0,1:T(2,128)} %param.24) | copy-start | bytes 6148
  202.4 6.0 %copy-start.8 = (f32[256]{0:T(256)S(1)}, f32[256]{0:T(256)}, u32[]{:S(2)}) copy-start(f32[256]{0:T(256)} %param.23) | copy-start | bytes 3076
  202.4 102.1 %all-to-all-start.2 = ((bf16[1,64,16,2048]{3,2,0,1:T(8,128)(2,1)}), bf16[1,64,16,2048]{3,2,0,1:T(8,128)(2,1)}, u32[]{:S(2)}, u32[]{:S(2)}) async-start(bf16[1,64,16,2048]{3,2,0,1:T(8,128)(2,1)} %convert_bitcast_fusion), calls=%async_computation.2 | async-start | bytes 8388608 | tf_op jit(solution)/shard_map/all_to_all | solution.py:87
  317.9 9.0 %copy-start.3 = (bf16[256,2048]{1,0:T(8,128)(2,1)S(1)}, bf16[256,2048]{1,0:T(8,128)(2,1)}, u32[]{:S(2)}) copy-start(bf16[256,2048]{1,0:T(8,128)(2,1)} %copy-done.2) | copy-start | bytes 3145732
Sparse Core Ops, SparseCore 0:
  9.2 59.3 all-gather.2
where the time goes:
time: 336 us; the launch traced here: 335 us
  waiting for transfers between devices  129 us (38%)
  blocking collectives  117 us (35%)
  local copies, waits for them, and re-layouts  28.5 us (8%)
  other arithmetic  18.2 us (5%)
  matrix products  17.6 us (5%)
  between operations  13.7 us (4%)
  starting transfers between devices  11.4 us (3%)
    all_to_all x1, blocking collectives, body(): lax.all_to_all(outgoing, 'sp', split_axis=1, concat_axis=1, tiled=True)  107 us
    all_to_all x1, waiting for transfers between devices, body(): lax.all_to_all(result, 'sp', split_axis=1, concat_axis=1, tiled=True)  96 us
    all_gather x1, waiting for transfers between devices, body(): lax.all_gather(out_weight, 'tp', axis=0, tiled=True)  18.5 us
    all_to_all x1, waiting for transfers between devices, body(): lax.all_to_all(mixed_out, 'tp', split_axis=0, concat_axis=1, tiled=True)  13.6 us
    all_gather x1, blocking collectives, body(): lax.all_gather(norm_gain, 'tp', axis=0, tiled=True)  9.99 us
    dot_general x1, matrix products, body(): jnp.einsum('esrf,efd->esrd', hidden, expert_down, preferred_element_type=...  9.96 us
    reduce_sum x1, other arithmetic, body(): jnp.sum(slot_out.astype(jnp.float32) * weights[:, :, None], axis=1)  8.96 us
    gather x1, local copies, waits for them, and re-layouts, body(): returned.reshape(-1, width)[position].reshape(tok_rows, top_count, width)  7.96 us
  transfers between devices with their start and end apart: 4, of which 3 were waited for; matrix products, arithmetic and copies ran while one was open for 4% of the time, Pallas kernels for 0%

commit v1 on v0

--- a/solution.py
+++ b/solution.py
@@ -4,6 +4,11 @@
 from jax.sharding import PartitionSpec as P
 
 EPSILON = 1e-06
+
+
+def gather_by_exchange(shard, axis, dim):
+    copies = jnp.concatenate([shard] * lax.axis_size(axis), axis=dim)
+    return lax.all_to_all(copies, axis, dim, dim, tiled=True)
 
 
 def from_behind(shard, axis, by):
@@ -46,7 +51,7 @@
     mixed_out = (gate_outer.astype(jnp.float32) * filtered).astype(jnp.bfloat16)
     gathered = lax.all_to_all(mixed_out, "tp", split_axis=0, concat_axis=1, tiled=True)
     full_weight, full_gain = (
-        lax.all_gather(out_weight, "tp", axis=0, tiled=True),
+        gather_by_exchange(out_weight, "tp", 0),
         lax.all_gather(norm_gain, "tp", axis=0, tiled=True),
     )
     normed = rms_norm(gathered, full_gain).astype(jnp.bfloat16)

time: 336 us -> 342 us (1.018)
  blocking collectives: 117 us -> 158 us
  waiting for transfers between devices: 129 us -> 104 us
  between operations: 13.7 us -> 0.25 us
  starting transfers between devices: 11.4 us -> 17.3 us
    all_gather x1, blocking collectives: 9.99 us -> 48.8 us  [body(): lax.all_gather(norm_gain, 'tp', axis=0, tiled=True)]
    all_gather x1 -> x0, waiting for transfers between devices: 18.5 us -> none  [body(): lax.all_gather(out_weight, 'tp', axis=0, tiled=True)]
    all_to_all x1, waiting for transfers between devices: 13.6 us -> 4.86 us  [body(): lax.all_to_all(mixed_out, 'tp', split_axis=0, concat_axis=1, tiled=True)]
    all_to_all x0 -> x1, starting transfers between devices: none -> 4.99 us  [gather_by_exchange(): return lax.all_to_all(copies, axis, dim, dim, tiled=True)]
    concatenate x0 -> x1, other arithmetic: none -> 4.11 us  [gather_by_exchange(): copies = jnp.concatenate([shard] * lax.axis_size(axis), axis=dim)]
  transfers between devices with their start and end apart: 4 -> 4, of which waited for: 3 -> 3; matrix products, arithmetic and copies ran while one was open for 4% -> 3% of each run, Pallas kernels for 0% -> 0%
where the time goes in v1:
time: 342 us
  blocking collectives  158 us (46%)
  waiting for transfers between devices  104 us (30%)
  local copies, waits for them, and re-layouts  26 us (8%)
  other arithmetic  18.9 us (6%)
  matrix products  17.6 us (5%)
  starting transfers between devices  17.3 us (5%)
    all_to_all x1, blocking collectives, body(): lax.all_to_all(outgoing, 'sp', split_axis=1, concat_axis=1, tiled=True)  109 us
    all_to_all x1, waiting for transfers between devices, body(): lax.all_to_all(result, 'sp', split_axis=1, concat_axis=1, tiled=True)  96 us
    all_gather x1, blocking collectives, body(): lax.all_gather(norm_gain, 'tp', axis=0, tiled=True)  48.8 us
    dot_general x1, matrix products, body(): jnp.einsum('esrf,efd->esrd', hidden, expert_down, preferred_element_type=...  9.96 us
    reduce_sum x1, other arithmetic, body(): jnp.sum(slot_out.astype(jnp.float32) * weights[:, :, None], axis=1)  8.96 us
    gather x1, local copies, waits for them, and re-layouts, body(): returned.reshape(-1, width)[position].reshape(tok_rows, top_count, width)  7.96 us
  transfers between devices with their start and end apart: 4, of which 3 were waited for; matrix products, arithmetic and copies ran while one was open for 3% of the time, Pallas kernels for 0%

profile of v1, /device:TPU:2, one launch (start us, length us, event | category | flops | bytes accessed | tf_op | source)
XLA Modules:
  0.0 341.6 jit_solution(7750521743143501529)
XLA Ops:
  0.0 1.5 convert_multiply_fusion.4
  1.5 1.9 collective-permute-start
  3.4 3.0 collective-permute-done
  6.4 1.2 fusion.26
  7.6 4.5 %all-to-all-start = ((bf16[4,256,256]{2,1,0:T(8,128)(2,1)}), bf16[4,256,256]{2,1,0:T(8,128)(2,1)S(1)}, u32[]{:S(2)}, u32[]{:S(2)}) async-start(bf16[4,256,256]{2,1,0:T(8,128)(2,1)} %bitcast.3), calls=%async_computation | async-start | bytes 1048576 | tf_op jit(solution)/shard_map/all_to_all | solution.py:52
  12.1 4.1 %pad_maximum_fusion = bf16[1024,2048]{1,0:T(8,128)(2,1)} fusion(bf16[256,2048]{1,0:T(8,128)(2,1)} %param.20), kind=kLoop, calls=%fused_computation.3 | loop fusion | flops 16777216 | bytes 5242880 | tf_op jit(solution)/shard_map/concatenate | solution.py:10
  16.2 4.9 %all-to-all-done = bf16[4,256,256]{2,1,0:T(8,128)(2,1)S(1)} async-done(((bf16[4,256,256]{2,1,0:T(8,128)(2,1)}), bf16[4,256,256]{2,1,0:T(8,128)(2,1)S(1)}, u32[]{:S(2)}, u32[]{:S(2)}) %all-to-all-start) | async-done | bytes 524320 | tf_op jit(solution)/shard_map/all_to_all | solution.py:52
  21.0 5.0 %all-to-all-start.1 = ((bf16[4,256,2048]{2,1,0:T(8,128)(2,1)}), bf16[4,256,2048]{2,1,0:T(8,128)(2,1)}, u32[]{:S(2)}, u32[]{:S(2)}) async-start(bf16[4,256,2048]{2,1,0:T(8,128)(2,1)} %bitcast.71), calls=%async_computation.1 | async-start | bytes 8388608 | tf_op jit(solution)/shard_map/all_to_all | solution.py:11
  26.5 48.8 %all-gather = bf16[4,1,256]{2,1,0:T(2,128)(2,1)S(1)} all-gather(bf16[1,1,256]{2,1,0:T(2,128)(2,1)S(1)} %reshape.156), channel_id=1, replica_groups=mesh['sp'=64,'tp'=4] {'tp'}, dimensions={0}, use_global_device_ids=true | all-gather | bytes 2560 | tf_op jit(solution)/shard_map/all_gather | solution.py:55
  75.3 1.2 reduce-window.6
  77.2 2.4 scatter_custom_fusion
  79.9 4.0 %fusion.6 = (f32[256]{0:T(256)S(1)}, bf16[256,2048]{1,0:T(8,128)(2,1)S(1)}) fusion(bf16[4,256,2048]{2,1,0:T(8,128)(2,1)} %all-to-all-done.1, bf16[4,256,256]{2,1,0:T(8,128)(2,1)S(1)} %all-to-all-done, f32[4,256]{1,0:T(4,128)S(1)} %bitcast.78, f32[256]{0:T(256)S(1)} %add_rsqrt_fusion.1, bf16[256,2048]{1,0:T(8,128)(2,1)} %param.14), kind=kOutput, calls=%fused_computation.16 | convolution fusion | flops 1077935872 | bytes 6821888 | tf_op jit(solution)/shard_map/dot_general | solution.py:58
  83.9 1.0 copy-done.2
  85.2 6.0 %gather_fusion = bf16[1024,2048]{1,0:T(8,128)(2,1)} fusion(bf16[257,2048]{1,0:T(8,128)(2,1)S(1)} %concatenate.11, s32[1024]{0:T(1024)S(1)} %fusion.40), kind=kCustom, calls=%fused_computation | custom fusion | bytes 8392704 | tf_op jit(solution)/shard_map/gather | solution.py:82
  91.3 108.9 %all_to_all.32 = bf16[1,64,16,2048]{3,2,0,1:T(8,128)(2,1)S(1)} all-to-all(bf16[1,64,16,2048]{3,2,0,1:T(8,128)(2,1)} %bitcast.70), channel_id=1, replica_groups=mesh['sp'=64,'tp'=4] {'sp'}, dimensions={1} | all-to-all | bytes 8388608 | tf_op jit(solution)/shard_map/all_to_all | solution.py:83
  200.2 2.0 copy-done.1
  202.1 3.7 %fusion.2 = f32[64,16,512]{2,1,0:T(8,128)} fusion(bf16[1,64,16,2048]{3,2,0,1:T(8,128)(2,1)S(1)} %all_to_all.32, bf16[1,2048,512]{2,1,0:T(8,128)(2,1)S(1)} %copy-done.10), kind=kOutput, calls=%fused_computation.6 | convolution fusion | flops 2147483648 | bytes 8388608 | tf_op jit(solution)/shard_map/esrd,edf->esrf/dot_general | solution.py:84
  205.9 10.0 %convert_bitcast_fusion = bf16[1,64,16,2048]{3,2,0,1:T(8,128)(2,1)} fusion(bf16[1,512,2048]{2,1,0:T(8,128)(2,1)S(1)} %copy-done, f32[64,16,512]{2,1,0:T(8,128)} %fusion.2, bf16[1,2048,512]{2,1,0:T(8,128)(2,1)} %param.26, bf16[1,64,16,2048]{3,2,0,1:T(8,128)(2,1)} %copy-done.1), kind=kOutput, calls=%fused_computation.9 | convolution fusion | flops 4300210176 | bytes 14680064 | tf_op jit(solution)/shard_map/esrf,efd->esrd/dot_general | solution.py:89
  215.8 5.9 %all-to-all-start.3 = ((bf16[1,64,16,2048]{3,2,0,1:T(8,128)(2,1)}), bf16[1,64,16,2048]{3,2,0,1:T(8,128)(2,1)}, u32[]{:S(2)}, u32[]{:S(2)}) async-start(bf16[1,64,16,2048]{3,2,0,1:T(8,128)(2,1)} %convert_bitcast_fusion), calls=%async_computation.3 | async-start | bytes 8388608 | tf_op jit(solution)/shard_map/all_to_all | solution.py:92
  221.9 96.0 %all-to-all-done.3 = bf16[1,64,16,2048]{3,2,0,1:T(8,128)(2,1)} async-done(((bf16[1,64,16,2048]{3,2,0,1:T(8,128)(2,1)}), bf16[1,64,16,2048]{3,2,0,1:T(8,128)(2,1)}, u32[]{:S(2)}, u32[]{:S(2)}) %all-to-all-start.3) | async-done | bytes 4194336 | tf_op jit(solution)/shard_map/all_to_all | solution.py:92
  317.9 8.0 %gather_fusion.1 = bf16[512,2048]{1,0:T(8,128)(2,1)} fusion(bf16[1024,2048]{1,0:T(8,128)(2,1)} %bitcast.21, s32[1024]{0:T(1024)S(1)} %pad_clamp_fusion), kind=kCustom, calls=%fused_computation.1 | custom fusion | bytes 4196352 | tf_op jit(solution)/shard_map/gather | solution.py:93
  325.9 5.4 %reshape.130 = f32[256,2,2048]{2,1,0:T(2,128)} reshape(bf16[512,2048]{1,0:T(8,128)(2,1)} %gather_fusion.1) | data formatting | bytes 6291456 | tf_op jit(solution)/shard_map/convert_element_type | solution.py:95
  331.3 9.0 %multiply_reduce_fusion = f32[256,2048]{1,0:T(8,128)S(1)} fusion(f32[256,2,2048]{2,1,0:T(2,128)} %reshape.130, f32[256,2]{1,0:T(8,128)S(1)} %copy.27), kind=kLoop, calls=%fused_computation.8 | loop fusion | flops 1572864 | bytes 6293504 | tf_op jit(solution)/shard_map/reduce_sum | solution.py:95
  340.3 1.3 fusion.9
  (51 shorter events, 2.0 us)
Async XLA Ops:
  0.0 205.9 %copy-start = (bf16[1,512,2048]{2,1,0:T(8,128)(2,1)S(1)}, bf16[1,512,2048]{2,1,0:T(8,128)(2,1)}, u32[]{:S(2)}) copy-start(bf16[1,512,2048]{2,1,0:T(8,128)(2,1)} %param.27) | copy-start | bytes 6291460
  0.0 3.4 %copy-start.7 = (bf16[3,256]{1,0:T(4,128)(2,1)S(1)}, bf16[3,256]{1,0:T(4,128)(2,1)}, u32[]{:S(2)}) copy-start(bf16[3,256]{1,0:T(4,128)(2,1)} %param.18) | copy-start | bytes 4612
  0.0 6.4 %copy-start.4 = (bf16[1024,256]{1,0:T(8,128)(2,1)S(1)}, bf16[1024,256]{1,0:T(8,128)(2,1)}, u32[]{:S(2)}) copy-start(bf16[1024,256]{1,0:T(8,128)(2,1)} %param.15) | copy-start | bytes 1572868
  1.5 4.9 %collective-permute-start = (f32[2,256]{1,0:T(2,128)S(1)}, f32[2,256]{1,0:T(2,128)S(1)}, u32[]{:S(2)}, u32[]{:S(2)}) collective-permute-start(f32[2,256]{1,0:T(2,128)S(1)} %slice.37), channel_id=1, source_target_pairs={{0,4},{4,8},{8,12},{12,16},{16,20},{20,24},{24,28},{28,32},{32,36}... | collective-permute-start | bytes 6152 | tf_op jit(solution)/shard_map/ppermute | solution.py:17
  7.6 13.4 %all-to-all-start = ((bf16[4,256,256]{2,1,0:T(8,128)(2,1)}), bf16[4,256,256]{2,1,0:T(8,128)(2,1)S(1)}, u32[]{:S(2)}, u32[]{:S(2)}) async-start(bf16[4,256,256]{2,1,0:T(8,128)(2,1)} %bitcast.3), calls=%async_computation | async-start | bytes 1048576 | tf_op jit(solution)/shard_map/all_to_all | solution.py:52
  21.0 5.0 %copy-start.5 = (s32[256,2]{0,1:T(2,128)S(1)}, s32[256,2]{0,1:T(2,128)}, u32[]{:S(2)}) copy-start(s32[256,2]{0,1:T(2,128)} %param.22) | copy-start | bytes 6148
  21.0 5.4 %copy-start.11 = (bf16[256]{0:T(256)(128)(2,1)S(1)}, bf16[256]{0:T(256)(128)(2,1)}, u32[]{:S(2)}) copy-start(bf16[256]{0:T(256)(128)(2,1)} %param.19) | copy-start | bytes 1540
  21.0 54.3 %copy-start.8 = (bf16[2048]{0:T(1024)(128)(2,1)S(1)}, bf16[2048]{0:T(1024)(128)(2,1)}, u32[]{:S(2)}) copy-start(bf16[2048]{0:T(1024)(128)(2,1)} %param.21) | copy-start | bytes 12292
  21.0 58.9 %all-to-all-start.1 = ((bf16[4,256,2048]{2,1,0:T(8,128)(2,1)}), bf16[4,256,2048]{2,1,0:T(8,128)(2,1)}, u32[]{:S(2)}, u32[]{:S(2)}) async-start(bf16[4,256,2048]{2,1,0:T(8,128)(2,1)} %bitcast.71), calls=%async_computation.1 | async-start | bytes 8388608 | tf_op jit(solution)/shard_map/all_to_all | solution.py:11
  83.9 1.0 copy-start.2
  91.3 110.9 %copy-start.10 = (bf16[1,2048,512]{2,1,0:T(8,128)(2,1)S(1)}, bf16[1,2048,512]{2,1,0:T(8,128)(2,1)}, u32[]{:S(2)}) copy-start(bf16[1,2048,512]{2,1,0:T(8,128)(2,1)} %param.25) | copy-start | bytes 6291460
  200.2 2.0 copy-start.1
  215.8 5.9 %copy-start.6 = (f32[256,2]{0,1:T(2,128)S(1)}, f32[256,2]{0,1:T(2,128)}, u32[]{:S(2)}) copy-start(f32[256,2]{0,1:T(2,128)} %param.24) | copy-start | bytes 6148
  215.8 5.9 %copy-start.9 = (f32[256]{0:T(256)S(1)}, f32[256]{0:T(256)}, u32[]{:S(2)}) copy-start(f32[256]{0:T(256)} %param.23) | copy-start | bytes 3076
  215.8 102.1 %all-to-all-start.3 = ((bf16[1,64,16,2048]{3,2,0,1:T(8,128)(2,1)}), bf16[1,64,16,2048]{3,2,0,1:T(8,128)(2,1)}, u32[]{:S(2)}, u32[]{:S(2)}) async-start(bf16[1,64,16,2048]{3,2,0,1:T(8,128)(2,1)} %convert_bitcast_fusion), calls=%async_computation.3 | async-start | bytes 8388608 | tf_op jit(solution)/shard_map/all_to_all | solution.py:92
  331.3 9.0 %copy-start.3 = (bf16[256,2048]{1,0:T(8,128)(2,1)S(1)}, bf16[256,2048]{1,0:T(8,128)(2,1)}, u32[]{:S(2)}) copy-start(bf16[256,2048]{1,0:T(8,128)(2,1)} %copy-done.2) | copy-start | bytes 3145732
